TPU v7x, 32 devices: a whole 2x2x4 slice. The times are simulated.
32 devices in a mesh: kv: 8 (over z, y), tp: 4 (over x, core).
Axes of the slice: x: 2, y: 2, z: 4, core: 2. Of those that a mesh axis runs over, the one named last changes fastest.
Arguments:
- tokens: bfloat16 [256, 4096], P(None, ('kv', 'tp')), may hold values from -60 to 60
- past_state: float32 [256, 16, 128, 128], P('kv', 'tp'), may hold values from -4 to 4
- pre_gain: float32 [4096], replicated, may hold values from 0.1 to 1.9
- pre_gate: bfloat16 [4096, 11264], P(None, ('kv', 'tp')), may hold values from -0.09375 to 0.09375
- pre_up: bfloat16 [4096, 11264], P(None, ('kv', 'tp')), may hold values from -0.09375 to 0.09375
- pre_down: bfloat16 [11264, 4096], P(('kv', 'tp')), may hold values from -0.109375 to 0.109375
- mix_gain: float32 [4096], replicated, may hold values from 0.1 to 1.9
- query_weight: bfloat16 [4096, 2048], P('kv', 'tp'), may hold values from -0.09375 to 0.09375
- forget_weight: bfloat16 [4096, 2048], P('kv', 'tp'), may hold values from -0.09375 to 0.09375
- value_weight: bfloat16 [4096, 2048], P('kv', 'tp'), may hold values from -0.09375 to 0.09375
- output_gate_weight: bfloat16 [4096, 2048], P('kv', 'tp'), may hold values from -0.09375 to 0.09375
- forget_floor: float32 [2048], P('tp'), may hold values from 0.02 to 0.9
- head_gain: float32 [128], replicated, may hold values from 0.1 to 1.9
- proj_out: bfloat16 [2048, 4096], P('tp', 'kv'), may hold values from -0.125 to 0.125
- post_gain: float32 [4096], replicated, may hold values from 0.1 to 1.9
- post_gate: bfloat16 [4096, 11264], P(None, ('kv', 'tp')), may hold values from -0.09375 to 0.09375
- post_up: bfloat16 [4096, 11264], P(None, ('kv', 'tp')), may hold values from -0.09375 to 0.09375
- post_down: bfloat16 [11264, 4096], P(('kv', 'tp')), may hold values from -0.109375 to 0.109375
Outputs:
- result: bfloat16 [256, 4096], P(None, ('kv', 'tp'))
- new_state: float32 [256, 16, 128, 128], P('kv', 'tp')
All inputs are finite; a program needn't handle non-finite values.
Results may differ from a plain program's by a relative error of at most 0.014.
Values may be sent and summed in bfloat16 or wider, within the bound.
A program may use at most 128 MiB of HBM per device.

v0:
```python
import jax
import jax.numpy as jnp
from jax import lax
from jax.sharding import PartitionSpec as P

D = 4096
epsilon = 1e-06


def half_inputs(activations, gain, w_gate, w_up):
    piece_float = lax.all_gather(activations, ("kv", "tp"), axis=1, tiled=True).astype(jnp.float32)
    normed = (piece_float * gain).astype(jnp.bfloat16)
    gate_acc = jnp.dot(normed, w_gate, preferred_element_type=jnp.float32)
    up_acc = jnp.dot(normed, w_up, preferred_element_type=jnp.float32)
    squares = jnp.sum(piece_float * piece_float, axis=1)
    row_scale = lax.rsqrt(squares / D + epsilon)[:, None]
    return (jax.nn.silu(row_scale * gate_acc) * (row_scale * up_acc)).astype(jnp.bfloat16)


def down_sum(hidden, w_down):
    return lax.psum_scatter(
        jnp.dot(hidden, w_down, preferred_element_type=jnp.float32),
        ("kv", "tp"),
        scatter_dimension=1,
        tiled=True,
    )


def per_device(
    tokens,
    past_state,
    pre_gain,
    pre_gate,
    pre_up,
    pre_down,
    mix_gain,
    query_weight,
    forget_weight,
    value_weight,
    output_gate_weight,
    forget_floor,
    head_gain,
    proj_out,
    post_gain,
    post_gate,
    post_up,
    post_down,
):
    whole_rows = lax.all_gather(tokens, ("kv", "tp"), axis=1, tiled=True)
    whole_float = whole_rows.astype(jnp.float32)
    row_scale = lax.rsqrt(jnp.mean(whole_float * whole_float, axis=1, keepdims=True) + epsilon)
    normed = (whole_float * pre_gain).astype(jnp.bfloat16)
    gate_pre = row_scale * jnp.dot(normed, pre_gate, preferred_element_type=jnp.float32)
    up_pre = row_scale * jnp.dot(normed, pre_up, preferred_element_type=jnp.float32)
    hidden = (jax.nn.silu(gate_pre) * up_pre).astype(jnp.bfloat16)
    kv_sums = lax.psum_scatter(
        jnp.dot(hidden, pre_down, preferred_element_type=jnp.float32).astype(jnp.bfloat16),
        "kv",
        scatter_dimension=1,
        tiled=True,
    )
    block_sum = lax.psum(kv_sums, "tp").astype(jnp.float32)
    block_width = block_sum.shape[1]
    block_old = lax.dynamic_slice_in_dim(
        whole_rows, lax.axis_index("kv") * block_width, block_width, 1
    )
    block_rows = (block_old.astype(jnp.float32) + 0.5 * block_sum).astype(jnp.bfloat16)
    own_width = block_width // lax.axis_size("tp")
    after_first = lax.dynamic_slice_in_dim(
        block_rows, lax.axis_index("tp") * own_width, own_width, 1
    )
    block_width = block_rows.shape[1]
    block_float = block_rows.astype(jnp.float32)
    block_gain = lax.dynamic_slice_in_dim(
        mix_gain, lax.axis_index("kv") * block_width, block_width, 0
    )
    squares = lax.psum(jnp.sum(block_float * block_float, axis=1), "kv")
    normed = (block_float * block_gain).astype(jnp.bfloat16)
    own_rows = past_state.shape[0]
    weight_list = (query_weight, forget_weight, value_weight, output_gate_weight)
    projected = lax.psum_scatter(
        jnp.concatenate(
            [
                jnp.dot(normed, weight_part, preferred_element_type=jnp.float32)
                for weight_part in weight_list
            ],
            axis=1,
        ).astype(jnp.bfloat16),
        "kv",
        scatter_dimension=0,
        tiled=True,
    ).astype(jnp.float32)
    own_squares = lax.dynamic_slice_in_dim(squares, lax.axis_index("kv") * own_rows, own_rows, 0)
    projected = projected * lax.rsqrt(own_squares / D + epsilon)[:, None]
    pre_query, pre_forget, pre_value, pre_gate_out = jnp.split(projected, 4, axis=1)
    local_heads = past_state.shape[1]
    head_width = past_state.shape[2]
    head_shape = (own_rows, local_heads, head_width)
    floors = forget_floor.reshape(local_heads, head_width)
    forget_heads = pre_forget.reshape(head_shape)
    forget = floors + (1.0 - floors) * jax.nn.sigmoid(forget_heads)
    written = (1.0 - floors) * jax.nn.sigmoid(-forget_heads)
    query_act = jax.nn.silu(pre_query.reshape(head_shape))
    value_act = pre_value.reshape(head_shape)
    new_state = (
        forget[:, :, :, None] * past_state + written[:, :, :, None] * value_act[:, :, None, :]
    )
    readout = jnp.einsum("bhkv,bhk->bhv", new_state, query_act, precision=lax.Precision.HIGHEST)
    readout = (
        readout
        * lax.rsqrt(jnp.mean(readout * readout, axis=2, keepdims=True) + epsilon)
        * head_gain
    )
    mixed_in = (
        readout.reshape(own_rows, local_heads * head_width) * jax.nn.silu(pre_gate_out)
    ).astype(jnp.bfloat16)
    partials = jnp.dot(
        lax.all_gather(mixed_in, "kv", axis=0, tiled=True),
        proj_out,
        preferred_element_type=jnp.float32,
    ).astype(jnp.bfloat16)
    mixed_sum = lax.psum_scatter(partials, "tp", scatter_dimension=1, tiled=True).astype(
        jnp.float32
    )
    second = (after_first.astype(jnp.float32) + mixed_sum).astype(jnp.bfloat16)
    hidden_two = half_inputs(second, post_gain, post_gate, post_up)
    result = (second.astype(jnp.float32) + 0.5 * down_sum(hidden_two, post_down)).astype(
        jnp.bfloat16
    )
    return (result, new_state)


def solution(mesh):
    placed = (
        P(None, ("kv", "tp")),
        P("kv", "tp", None, None),
        P(),
        P(None, ("kv", "tp")),
        P(None, ("kv", "tp")),
        P(("kv", "tp"), None),
        P(),
        P("kv", "tp"),
        P("kv", "tp"),
        P("kv", "tp"),
        P("kv", "tp"),
        P("tp"),
        P(),
        P("tp", "kv"),
        P(),
        P(None, ("kv", "tp")),
        P(None, ("kv", "tp")),
        P(("kv", "tp"), None),
    )
    return jax.shard_map(
        per_device,
        mesh=mesh,
        in_specs=placed,
        out_specs=(P(None, ("kv", "tp")), P("kv", "tp", None, None)),
        check_vma=False,
    )
```

profile of v0, /device:TPU:0, one launch (start us, length us, event | category | flops | bytes accessed | tf_op | source)
XLA Modules:
  0.0 548.7 jit_solution(15226853268982632663)
XLA Ops:
  8.0 58.6 %all-gather.3.cloned.1.call-done = bf16[256,4096]{1,0:T(8,128)(2,1)} async-done(((bf16[256,128]{1,0:T(8,128)(2,1)}), bf16[256,4096]{1,0:T(8,128)(2,1)}) %all-gather.3.cloned.1.call-update) | async-done | bytes 2097168 | tf_op jit(solution)/shard_map/all_gather | solution.py:49
  66.6 2.1 fusion
  68.7 3.4 fusion.12
  72.1 7.5 %convolution_convert_fusion = bf16[256,4096]{1,0:T(8,128)(2,1)} fusion(bf16[352,4096]{1,0:T(8,128)(2,1)S(1)} %copy-done, bf16[4096,352]{0,1:T(8,128)(2,1)} %param.22, bf16[256,4096]{1,0:T(8,128)(2,1)} %all-gather.3.cloned.1.call-done, f32[4096]{0:T(1024)S(1)} %copy-done.7, f32[256,352]{0,1:T(8,128)S(1)} %fusion.12, f32[256]{0:T(256)S(1)} %add_rsqrt_fusion.2), kind=kOutput, calls=%fused_computation.5 | convolution fusion | flops 1481220096 | bytes 10339328 | tf_op jit(solution)/shard_map/dot_general | solution.py:57
  79.7 68.1 %reduce-scatter.7.cloned.1.call-done = bf16[256,512]{1,0:T(8,128)(2,1)} async-done(((bf16[256,4096]{1,0:T(8,128)(2,1)}), bf16[256,512]{1,0:T(8,128)(2,1)}) %reduce-scatter.7.cloned.1.call-update) | async-done | bytes 262160 | tf_op jit(solution)/shard_map/reduce_scatter | solution.py:56
  147.8 0.8 dynamic_slice.14
  148.6 32.8 %all-reduce.2.cloned.1.call-done = bf16[256,512]{1,0:T(8,128)(2,1)} async-done(((bf16[256,512]{1,0:T(8,128)(2,1)}), bf16[256,512]{1,0:T(8,128)(2,1)}) %all-reduce.2.cloned.1.call-update) | async-done | bytes 262160 | tf_op jit(solution)/shard_map/psum | solution.py:62
  181.4 1.2 fusion.42
  182.6 1.3 convolution_convert_fusion.3
  183.9 1.3 convolution_convert_fusion.2
  185.3 1.3 convolution_convert_fusion.4
  186.6 1.3 convolution_convert_fusion.5
  188.0 1.1 pad_maximum_fusion
  189.2 21.6 %psum.15 = f32[256]{0:T(256)S(1)} all-reduce(f32[256]{0:T(256)S(1)} %get-tuple-element.2), channel_id=1, replica_groups=mesh['kv'=8,'tp'=4] {'kv'}, use_global_device_ids=true, to_apply=%region_5.6 | all-reduce | flops 256 | bytes 2048 | tf_op jit(solution)/shard_map/psum | solution.py:77
  210.8 42.6 %reduce-scatter.9.cloned.1.call-done = bf16[32,2048]{1,0:T(8,128)(2,1)} async-done(((bf16[256,2048]{1,0:T(8,128)(2,1)}), bf16[32,2048]{1,0:T(8,128)(2,1)}) %reduce-scatter.9.cloned.1.call-update) | async-done | bytes 131088 | tf_op jit(solution)/shard_map/reduce_scatter | solution.py:81
  253.5 1.0 convert_multiply_fusion.6
  255.8 0.9 divide_multiply_fusion
  257.3 0.9 mul.203
  258.2 1.5 div.63
  259.6 0.9 multiply_add_fusion.1
  260.5 8.2 %multiply_add_fusion = f32[32,4,128,128]{3,2,1,0:T(8,128)S(1)} fusion(f32[32,4,128,128]{3,2,1,0:T(8,128)} %param.19, f32[32,4,128]{2,1,0:T(4,128)S(1)} %mul.203, f32[32,4,128]{2,1,0:T(4,128)S(1)} %bitcast.39, f32[32,4,128]{2,1,0:T(4,128)S(1)} %bitcast.38), kind=kLoop, calls=%fused_computation | loop fusion | flops 6291456 | bytes 16973824 | tf_op jit(solution)/shard_map/add | solution.py:106
  268.8 7.2 %fusion.65 = f32[32,4,1,128]{3,2,1,0:T(1,128)S(1)} fusion(f32[32,4,128,128]{3,2,1,0:T(8,128)S(1)} %multiply_add_fusion, f32[32,4,128,1]{2,3,1,0:T(1,128)S(1)} %bitcast.37), kind=kOutput, calls=%fused_computation.68 | convolution fusion | flops 25165824 | bytes 8519680 | tf_op jit(solution)/shard_map/bhkv,bhk->bhv/dot_general | solution.py:108
  276.3 30.8 %all_gather.10 = bf16[256,512]{1,0:T(8,128)(2,1)S(1)} all-gather(bf16[32,512]{1,0:T(8,128)(2,1)S(1)} %fusion.61), channel_id=1, replica_groups=mesh['kv'=8,'tp'=4] {'kv'}, dimensions={0}, use_global_device_ids=true | all-gather | bytes 294912 | tf_op jit(solution)/shard_map/all_gather | solution.py:118
  307.4 0.8 copy.22
  308.3 19.2 %reduce-scatter.13.cloned.1.call-done = bf16[128,256]{1,0:T(8,128)(2,1)} async-done(((bf16[512,256]{1,0:T(8,128)(2,1)}), bf16[128,256]{1,0:T(8,128)(2,1)}) %reduce-scatter.13.cloned.1.call-update) | async-done | bytes 65552
  327.5 0.9 copy.23
  329.4 54.4 %all-gather.5.cloned.1.call-done = bf16[256,4096]{1,0:T(8,128)(2,1)} async-done(((bf16[256,128]{1,0:T(8,128)(2,1)}), bf16[256,4096]{1,0:T(8,128)(2,1)}) %all-gather.5.cloned.1.call-update) | async-done | bytes 2097168 | tf_op jit(solution)/shard_map/all_gather | solution.py:11
  383.8 2.1 fusion.2
  385.9 3.4 fusion.18
  389.3 8.9 %fusion.37 = f32[256,4096]{1,0:T(8,128)} fusion(bf16[352,4096]{1,0:T(8,128)(2,1)} %param.35, bf16[4096,352]{0,1:T(8,128)(2,1)} %param.34, bf16[256,4096]{1,0:T(8,128)(2,1)} %all-gather.5.cloned.1.call-done, f32[4096]{0:T(1024)S(1)} %copy-done.4, f32[256,352]{0,1:T(8,128)S(1)} %fusion.18, f32[256]{0:T(256)S(1)} %add_rsqrt_fusion.1), kind=kOutput, calls=%fused_computation.27 | convolution fusion | flops 1480171520 | bytes 12436480 | tf_op jit(solution)/shard_map/dot_general | solution.py:22
  398.3 142.1 %reduce-scatter.11.cloned.1.call-done = f32[256,128]{1,0:T(8,128)} async-done(((f32[256,4096]{1,0:T(8,128)}), f32[256,128]{1,0:T(8,128)}) %reduce-scatter.11.cloned.1.call-update) | async-done | bytes 131088 | tf_op jit(solution)/shard_map/reduce_scatter | solution.py:21
  540.3 1.6 add_convert_fusion.1
  (45 shorter events, 4.6 us)
Async XLA Ops:
  7.2 65.0 %copy-start = (bf16[352,4096]{1,0:T(8,128)(2,1)S(1)}, bf16[352,4096]{1,0:T(8,128)(2,1)}, u32[]{:S(2)}) copy-start(bf16[352,4096]{1,0:T(8,128)(2,1)} %param.23) | copy-start | bytes 8650756
  7.2 59.4 %all-gather.3.cloned.1.call-start = ((), (), s32[]{:S(2)}) async-start(), calls=%async_computation.4 | async-start | bytes 2162688 | tf_op jit(solution)/shard_map/all_gather | solution.py:49
  7.9 139.8 %reduce-scatter.7.cloned.1.call-start = ((), (), s32[]{:S(2)}) async-start(), calls=%async_computation.5 | async-start | bytes 2359296 | tf_op jit(solution)/shard_map/reduce_scatter | solution.py:56
  68.7 3.5 copy-start.7
  79.6 101.7 %all-reduce.2.cloned.1.call-start = ((), (), s32[]{:S(2)}) async-start(), calls=%async_computation.6 | async-start | bytes 524288 | tf_op jit(solution)/shard_map/psum | solution.py:62
  147.8 105.7 %reduce-scatter.9.cloned.1.call-start = ((), (), s32[]{:S(2)}) async-start(), calls=%async_computation.7 | async-start | bytes 1179648 | tf_op jit(solution)/shard_map/reduce_scatter | solution.py:81
  185.3 3.9 copy-start.5
  189.1 138.4 %reduce-scatter.13.cloned.1.call-start = ((), (), s32[]{:S(2)}) async-start(), calls=%async_computation.10 | async-start | bytes 327680
  268.8 7.2 %copy-start.1 = (f32[32,4,128,128]{3,2,1,0:T(8,128)}, f32[32,4,128,128]{3,2,1,0:T(8,128)S(1)}, u32[]{:S(2)}) copy-start(f32[32,4,128,128]{3,2,1,0:T(8,128)S(1)} %multiply_add_fusion) | copy-start | bytes 25165828
  268.8 7.3 %copy-start.6 = (f32[128]{0:T(128)S(1)}, f32[128]{0:T(128)}, u32[]{:S(2)}) copy-start(f32[128]{0:T(128)} %param.30) | copy-start | bytes 1540
  268.8 38.3 %copy-start.3 = (bf16[512,512]{1,0:T(8,128)(2,1)S(1)}, bf16[512,512]{1,0:T(8,128)(2,1)}, u32[]{:S(2)}) copy-start(bf16[512,512]{1,0:T(8,128)(2,1)} %param.31) | copy-start | bytes 1572868
  276.0 109.9 %copy-start.4 = (f32[4096]{0:T(1024)S(1)}, f32[4096]{0:T(1024)}, u32[]{:S(2)}) copy-start(f32[4096]{0:T(1024)} %param.32) | copy-start | bytes 49156
  308.3 75.5 %all-gather.5.cloned.1.call-start = ((), (), s32[]{:S(2)}) async-start(), calls=%async_computation.8 | async-start | bytes 2162688 | tf_op jit(solution)/shard_map/all_gather | solution.py:11
  329.1 211.2 %reduce-scatter.11.cloned.1.call-start = ((), (), s32[]{:S(2)}) async-start(), calls=%async_computation.9 | async-start | bytes 4325376 | tf_op jit(solution)/shard_map/reduce_scatter | solution.py:21
  398.2 142.1 %copy-start.2 = (bf16[256,128]{1,0:T(8,128)(2,1)S(1)}, bf16[256,128]{1,0:T(8,128)(2,1)}, u32[]{:S(2)}) copy-start(bf16[256,128]{1,0:T(8,128)(2,1)} %add_convert_fusion.2) | copy-start | bytes 196612
Sparse Core Ops, SparseCore 0:
  10.8 55.6 all-gather.2
  79.7 67.9 reduce-scatter.6
  150.1 31.2 all-reduce.1
  189.2 64.1 reduce-scatter.8
  308.4 19.0 reduce-scatter.12
  330.8 52.9 all-gather.4
  398.4 141.8 reduce-scatter.10
where the time goes:
time: 550 us; the launch traced here: 549 us
  waiting for transfers between devices  418 us (76%)
  blocking collectives  52.4 us (10%)
  matrix products  36.1 us (7%)
  other arithmetic  20.7 us (4%)
  between operations  14.4 us (3%)
  local copies, waits for them, and re-layouts  6.21 us (1%)
    reduce_scatter x1, waiting for transfers between devices, down_sum(): lax.psum_scatter(jnp.dot(hidden, w_down, preferred_element_type=jnp.float...  142 us
    reduce_scatter x1, waiting for transfers between devices, per_device(): lax.psum_scatter(jnp.dot(hidden, pre_down, preferred_element_type=jnp.flo...  68.1 us
    all_gather x1, waiting for transfers between devices, per_device(): whole_rows = lax.all_gather(tokens, ('kv', 'tp'), axis=1, tiled=True)  58.6 us
    all_gather x1, waiting for transfers between devices, half_inputs(): lax.all_gather(activations, ('kv', 'tp'), axis=1, tiled=True)  54.4 us
    reduce_scatter x1, waiting for transfers between devices, per_device(): lax.psum_scatter(jnp.concatenate([jnp.dot(normed, weight_part, preferred_...  42.6 us
    psum x1, waiting for transfers between devices, per_device(): block_sum = lax.psum(kv_sums, 'tp').astype(jnp.float32)  32.8 us
    all_gather x1, blocking collectives, per_device(): lax.all_gather(mixed_in, 'kv', axis=0, tiled=True)  30.8 us
    psum x1, blocking collectives, per_device(): squares = lax.psum(jnp.sum(block_float * block_float, axis=1), 'kv')  21.6 us
  transfers between devices with their start and end apart: 7, of which 7 were waited for; matrix products, arithmetic and copies ran while one was open for 0% of the time, Pallas kernels for 0%

commit v1 on v0

--- a/solution.py
+++ b/solution.py
@@ -59,7 +59,7 @@
         scatter_dimension=1,
         tiled=True,
     )
-    block_sum = lax.psum(kv_sums, "tp").astype(jnp.float32)
+    block_sum = jnp.sum(lax.all_gather(kv_sums, "tp"), axis=0).astype(jnp.float32)
     block_width = block_sum.shape[1]
     block_old = lax.dynamic_slice_in_dim(
         whole_rows, lax.axis_index("kv") * block_width, block_width, 1

time: 550 us -> 532 us (0.967)
  waiting for transfers between devices: 418 us -> 402 us
    psum x1 -> x0, waiting for transfers between devices: 32.8 us -> none  [per_device(): block_sum = lax.psum(kv_sums, 'tp').astype(jnp.float32)]
    all_gather x0 -> x1, waiting for transfers between devices: none -> 16.4 us  [per_device(): lax.all_gather(kv_sums, 'tp')]
where the time goes in v1:
time: 532 us; the launch traced here: 531 us
  waiting for transfers between devices  402 us (76%)
  blocking collectives  52.4 us (10%)
  matrix products  34 us (6%)
  other arithmetic  22.2 us (4%)
  between operations  14.4 us (3%)
  local copies, waits for them, and re-layouts  6.24 us (1%)
    reduce_scatter x1, waiting for transfers between devices, down_sum(): lax.psum_scatter(jnp.dot(hidden, w_down, preferred_element_type=jnp.float...  142 us
    reduce_scatter x1, waiting for transfers between devices, per_device(): lax.psum_scatter(jnp.dot(hidden, pre_down, preferred_element_type=jnp.flo...  68.1 us
    all_gather x1, waiting for transfers between devices, per_device(): whole_rows = lax.all_gather(tokens, ('kv', 'tp'), axis=1, tiled=True)  58.6 us
    all_gather x1, waiting for transfers between devices, half_inputs(): lax.all_gather(activations, ('kv', 'tp'), axis=1, tiled=True)  54.4 us
    reduce_scatter x1, waiting for transfers between devices, per_device(): lax.psum_scatter(jnp.concatenate([jnp.dot(normed, weight_part, preferred_...  42.6 us
    all_gather x1, blocking collectives, per_device(): lax.all_gather(mixed_in, 'kv', axis=0, tiled=True)  30.9 us
    psum x1, blocking collectives, per_device(): squares = lax.psum(jnp.sum(block_float * block_float, axis=1), 'kv')  21.5 us
    unnamed x8, waiting for transfers between devices  19.7 us
  transfers between devices with their start and end apart: 7, of which 7 were waited for; matrix products, arithmetic and copies ran while one was open for 0% of the time, Pallas kernels for 0%

profile of v1, /device:TPU:0, one launch (start us, length us, event | category | flops | bytes accessed | tf_op | source)
XLA Modules:
  0.0 531.4 jit_solution(10207667071552576225)
XLA Ops:
  7.2 0.7 all-gather.5.cloned.1.call-update
  8.0 58.6 %all-gather.5.cloned.1.call-done = bf16[256,4096]{1,0:T(8,128)(2,1)} async-done(((bf16[256,128]{1,0:T(8,128)(2,1)}), bf16[256,4096]{1,0:T(8,128)(2,1)}) %all-gather.5.cloned.1.call-update) | async-done | bytes 2097168 | tf_op jit(solution)/shard_map/all_gather | solution.py:49
  66.6 2.1 fusion
  68.7 3.4 fusion.12
  72.1 7.5 %convolution_convert_fusion = bf16[256,4096]{1,0:T(8,128)(2,1)} fusion(bf16[352,4096]{1,0:T(8,128)(2,1)S(1)} %copy-done, bf16[4096,352]{0,1:T(8,128)(2,1)} %param.22, bf16[256,4096]{1,0:T(8,128)(2,1)} %all-gather.5.cloned.1.call-done, f32[4096]{0:T(1024)S(1)} %copy-done.9, f32[256,352]{0,1:T(8,128)S(1)} %fusion.12, f32[256]{0:T(256)S(1)} %add_rsqrt_fusion.2), kind=kOutput, calls=%fused_computation.5 | convolution fusion | flops 1481220096 | bytes 10339328 | tf_op jit(solution)/shard_map/dot_general | solution.py:57
  79.7 68.1 %reduce-scatter.7.cloned.1.call-done = bf16[256,512]{1,0:T(8,128)(2,1)} async-done(((bf16[256,4096]{1,0:T(8,128)(2,1)}), bf16[256,512]{1,0:T(8,128)(2,1)}) %reduce-scatter.7.cloned.1.call-update) | async-done | bytes 262160 | tf_op jit(solution)/shard_map/reduce_scatter | solution.py:56
  147.8 0.8 dynamic_slice.14
  148.6 16.4 %all-gather.9.cloned.1.call-done = bf16[1024,512]{1,0:T(8,128)(2,1)} async-done(((bf16[256,512]{1,0:T(8,128)(2,1)}), bf16[1024,512]{1,0:T(8,128)(2,1)}) %all-gather.9.cloned.1.call-update) | async-done | bytes 1048592 | tf_op jit(solution)/shard_map/all_gather | solution.py:62
  165.0 1.5 reduce_sum.49
  166.5 1.2 fusion.42
  167.7 1.3 convolution_convert_fusion.3
  169.1 1.3 convolution_convert_fusion.2
  171.1 1.1 pad_maximum_fusion
  172.3 21.5 %psum.7 = f32[256]{0:T(256)S(1)} all-reduce(f32[256]{0:T(256)S(1)} %get-tuple-element.2), channel_id=1, replica_groups=mesh['kv'=8,'tp'=4] {'kv'}, use_global_device_ids=true, to_apply=%region_5.6 | all-reduce | flops 256 | bytes 2048 | tf_op jit(solution)/shard_map/psum | solution.py:77
  193.9 42.6 %reduce-scatter.9.cloned.1.call-done = bf16[32,2048]{1,0:T(8,128)(2,1)} async-done(((bf16[256,2048]{1,0:T(8,128)(2,1)}), bf16[32,2048]{1,0:T(8,128)(2,1)}) %reduce-scatter.9.cloned.1.call-update) | async-done | bytes 131088 | tf_op jit(solution)/shard_map/reduce_scatter | solution.py:81
  236.5 1.0 convert_multiply_fusion.6
  238.8 0.9 divide_multiply_fusion
  240.3 0.9 mul.203
  241.2 1.5 div.63
  242.7 0.9 multiply_add_fusion.1
  243.6 8.2 %multiply_add_fusion = f32[32,4,128,128]{3,2,1,0:T(8,128)S(1)} fusion(f32[32,4,128,128]{3,2,1,0:T(8,128)} %param.19, f32[32,4,128]{2,1,0:T(4,128)S(1)} %mul.203, f32[32,4,128]{2,1,0:T(4,128)S(1)} %bitcast.41, f32[32,4,128]{2,1,0:T(4,128)S(1)} %bitcast.40), kind=kLoop, calls=%fused_computation | loop fusion | flops 6291456 | bytes 16973824 | tf_op jit(solution)/shard_map/add | solution.py:106
  251.8 7.2 %fusion.65 = f32[32,4,1,128]{3,2,1,0:T(1,128)S(1)} fusion(f32[32,4,128,128]{3,2,1,0:T(8,128)S(1)} %multiply_add_fusion, f32[32,4,128,1]{2,3,1,0:T(1,128)S(1)} %bitcast.39), kind=kOutput, calls=%fused_computation.68 | convolution fusion | flops 25165824 | bytes 8519680 | tf_op jit(solution)/shard_map/bhkv,bhk->bhv/dot_general | solution.py:108
  259.3 30.9 %all_gather.18 = bf16[256,512]{1,0:T(8,128)(2,1)S(1)} all-gather(bf16[32,512]{1,0:T(8,128)(2,1)S(1)} %fusion.61), channel_id=1, replica_groups=mesh['kv'=8,'tp'=4] {'kv'}, dimensions={0}, use_global_device_ids=true | all-gather | bytes 294912 | tf_op jit(solution)/shard_map/all_gather | solution.py:118
  290.5 0.8 copy.22
  291.4 18.9 %reduce-scatter.13.cloned.1.call-done = bf16[128,256]{1,0:T(8,128)(2,1)} async-done(((bf16[512,256]{1,0:T(8,128)(2,1)}), bf16[128,256]{1,0:T(8,128)(2,1)}) %reduce-scatter.13.cloned.1.call-update) | async-done | bytes 65552
  310.3 0.9 copy.23
  312.2 54.4 %all-gather.7.cloned.1.call-done = bf16[256,4096]{1,0:T(8,128)(2,1)} async-done(((bf16[256,128]{1,0:T(8,128)(2,1)}), bf16[256,4096]{1,0:T(8,128)(2,1)}) %all-gather.7.cloned.1.call-update) | async-done | bytes 2097168 | tf_op jit(solution)/shard_map/all_gather | solution.py:11
  366.6 2.1 fusion.2
  368.7 3.4 fusion.18
  372.1 8.9 %fusion.37 = f32[256,4096]{1,0:T(8,128)} fusion(bf16[352,4096]{1,0:T(8,128)(2,1)} %param.35, bf16[4096,352]{0,1:T(8,128)(2,1)} %param.34, bf16[256,4096]{1,0:T(8,128)(2,1)} %all-gather.7.cloned.1.call-done, f32[4096]{0:T(1024)S(1)} %copy-done.6, f32[256,352]{0,1:T(8,128)S(1)} %fusion.18, f32[256]{0:T(256)S(1)} %add_rsqrt_fusion.1), kind=kOutput, calls=%fused_computation.27 | convolution fusion | flops 1480171520 | bytes 12436480 | tf_op jit(solution)/shard_map/dot_general | solution.py:22
  381.1 141.9 %reduce-scatter.11.cloned.1.call-done = f32[256,128]{1,0:T(8,128)} async-done(((f32[256,4096]{1,0:T(8,128)}), f32[256,128]{1,0:T(8,128)}) %reduce-scatter.11.cloned.1.call-update) | async-done | bytes 131088 | tf_op jit(solution)/shard_map/reduce_scatter | solution.py:21
  523.0 1.6 add_convert_fusion.1
  (50 shorter events, 4.5 us)
Async XLA Ops:
  7.2 65.0 %copy-start = (bf16[352,4096]{1,0:T(8,128)(2,1)S(1)}, bf16[352,4096]{1,0:T(8,128)(2,1)}, u32[]{:S(2)}) copy-start(bf16[352,4096]{1,0:T(8,128)(2,1)} %param.23) | copy-start | bytes 8650756
  7.2 59.4 %all-gather.5.cloned.1.call-start = ((), (), s32[]{:S(2)}) async-start(), calls=%async_computation.4 | async-start | bytes 2162688 | tf_op jit(solution)/shard_map/all_gather | solution.py:49
  7.9 139.8 %reduce-scatter.7.cloned.1.call-start = ((), (), s32[]{:S(2)}) async-start(), calls=%async_computation.5 | async-start | bytes 2359296 | tf_op jit(solution)/shard_map/reduce_scatter | solution.py:56
  68.7 3.5 copy-start.9
  79.6 85.4 %all-gather.9.cloned.1.call-start = ((), (), s32[]{:S(2)}) async-start(), calls=%async_computation.9 | async-start | bytes 1310720 | tf_op jit(solution)/shard_map/all_gather | solution.py:62
  147.8 88.7 %reduce-scatter.9.cloned.1.call-start = ((), (), s32[]{:S(2)}) async-start(), calls=%async_computation.6 | async-start | bytes 1179648 | tf_op jit(solution)/shard_map/reduce_scatter | solution.py:81
  166.5 4.0 copy-start.3
  166.5 4.3 copy-start.4
  170.4 1.8 copy-start.7
  172.2 138.1 %reduce-scatter.13.cloned.1.call-start = ((), (), s32[]{:S(2)}) async-start(), calls=%async_computation.10 | async-start | bytes 327680
  251.8 7.2 %copy-start.1 = (f32[32,4,128,128]{3,2,1,0:T(8,128)}, f32[32,4,128,128]{3,2,1,0:T(8,128)S(1)}, u32[]{:S(2)}) copy-start(f32[32,4,128,128]{3,2,1,0:T(8,128)S(1)} %multiply_add_fusion) | copy-start | bytes 25165828
  251.8 7.3 %copy-start.8 = (f32[128]{0:T(128)S(1)}, f32[128]{0:T(128)}, u32[]{:S(2)}) copy-start(f32[128]{0:T(128)} %param.30) | copy-start | bytes 1540
  251.8 38.4 %copy-start.5 = (bf16[512,512]{1,0:T(8,128)(2,1)S(1)}, bf16[512,512]{1,0:T(8,128)(2,1)}, u32[]{:S(2)}) copy-start(bf16[512,512]{1,0:T(8,128)(2,1)} %param.31) | copy-start | bytes 1572868
  259.0 109.7 %copy-start.6 = (f32[4096]{0:T(1024)S(1)}, f32[4096]{0:T(1024)}, u32[]{:S(2)}) copy-start(f32[4096]{0:T(1024)} %param.32) | copy-start | bytes 49156
  291.3 75.3 %all-gather.7.cloned.1.call-start = ((), (), s32[]{:S(2)}) async-start(), calls=%async_computation.7 | async-start | bytes 2162688 | tf_op jit(solution)/shard_map/all_gather | solution.py:11
  311.9 211.1 %reduce-scatter.11.cloned.1.call-start = ((), (), s32[]{:S(2)}) async-start(), calls=%async_computation.8 | async-start | bytes 4325376 | tf_op jit(solution)/shard_map/reduce_scatter | solution.py:21
  381.1 141.9 %copy-start.2 = (bf16[256,128]{1,0:T(8,128)(2,1)S(1)}, bf16[256,128]{1,0:T(8,128)(2,1)}, u32[]{:S(2)}) copy-start(bf16[256,128]{1,0:T(8,128)(2,1)} %add_convert_fusion.2) | copy-start | bytes 196612
Sparse Core Ops, SparseCore 0:
  10.8 55.6 all-gather.4
  79.7 67.9 reduce-scatter.6
  149.3 15.6 all-gather.8
  172.3 64.0 reduce-scatter.8
  291.5 18.7 reduce-scatter.12
  313.6 52.9 all-gather.6
  381.2 141.7 reduce-scatter.10
